TPU v7x, 32 devices: a whole 2x2x4 slice. The times are simulated.
32 devices in a mesh: ep: 16 (over z, y, x), tp: 2 (over core).
Axes of the slice: x: 2, y: 2, z: 4, core: 2. Of those that a mesh axis runs over, the one named last changes fastest.
Arguments:
- tokens: bfloat16 [64, 4096], P('ep'), may hold values from -6 to 6
- memory: float32 [64, 8, 256, 512], P('ep', 'tp'), may hold values from -6 to 6
- normalizer: float32 [64, 8, 256], P('ep', 'tp'), may hold values from -6 to 6
- stabilizer: float32 [64, 8], P('ep', 'tp'), may hold values from -4 to 4
- norm_gain: float32 [4096], replicated, may hold values from 0.1 to 1.9
- w_query: bfloat16 [4096, 8, 256], P(None, 'tp', 'ep'), may hold values from -0.09375 to 0.09375
- w_key: bfloat16 [4096, 8, 256], P(None, 'tp', 'ep'), may hold values from -0.09375 to 0.09375
- w_value: bfloat16 [4096, 8, 512], P(None, 'tp', 'ep'), may hold values from -0.09375 to 0.09375
- w_outgate: bfloat16 [4096, 8, 512], P(None, 'tp', 'ep'), may hold values from -0.09375 to 0.09375
- w_input: bfloat16 [4096, 8], P(None, 'tp'), may hold values from -0.09375 to 0.09375
- w_forget: bfloat16 [4096, 8], P(None, 'tp'), may hold values from -0.09375 to 0.09375
- forget_bias: float32 [8], P('tp'), may hold values from 0 to 4
- w_out: bfloat16 [4096, 4096], P('tp', 'ep'), may hold values from -0.09375 to 0.09375
- ffn_gain: float32 [4096], replicated, may hold values from 0.1 to 1.9
- w_gate: bfloat16 [16, 4096, 512], P('ep', None, 'tp'), may hold values from -0.09375 to 0.09375
- w_up: bfloat16 [16, 4096, 512], P('ep', None, 'tp'), may hold values from -0.09375 to 0.09375
- w_down: bfloat16 [16, 512, 4096], P('ep', 'tp'), may hold values from -0.25 to 0.25
- expert_ids: int32 [64, 2], P('ep'), may hold values from 0 to 15, as said below
- route_weights: float32 [64, 2], P('ep'), may hold values from 0.1 to 1
Outputs:
- out: bfloat16 [64, 4096], P('ep')
- memory_next: float32 [64, 8, 256, 512], P('ep', 'tp')
- normalizer_next: float32 [64, 8, 256], P('ep', 'tp')
- stabilizer_next: float32 [64, 8], P('ep', 'tp')
Inputs may be any that keep to these rules, and one draw needn't show every extreme that they name: `expert_ids`: the 2 experts of a token differ and lie in one group of 8 consecutive experts. Beyond that, any choice is allowed: for instance, all 4 tokens of one index of ep may name the same expert.
All inputs are finite; a program needn't handle non-finite values.
Results may differ from a plain program's by a relative error of at most 0.013.
Values may be sent and summed in bfloat16 or wider, within the bound.
A program may use at most 128 MiB of HBM per device.

v0:
```python
import jax
import jax.numpy as jnp
from jax import lax
from jax.sharding import PartitionSpec as P


def rms_scale(values, gain):
    return values * lax.rsqrt(jnp.mean(values * values, axis=-1, keepdims=True) + 1e-06) * gain


def product(left, right):
    return jnp.dot(left, right, preferred_element_type=jnp.float32)


def rounded_term(values):
    return lax.optimization_barrier(values.astype(jnp.bfloat16)).astype(jnp.float32)


def body(
    tokens,
    memory,
    normalizer,
    stabilizer,
    norm_gain,
    w_query,
    w_key,
    w_value,
    w_outgate,
    w_input,
    w_forget,
    forget_bias,
    w_out,
    ffn_gain,
    w_gate,
    w_up,
    w_down,
    expert_ids,
    route_weights,
):
    seqs, width = tokens.shape
    heads, key_size, value_size = (memory.shape[1], memory.shape[2], memory.shape[3])
    value_width = heads * value_size
    key_piece = w_query.shape[2]
    value_piece = w_value.shape[2]
    query_cols = w_query.reshape(width, heads * key_piece)
    key_cols = w_key.reshape(width, heads * key_piece)
    value_cols = w_value.reshape(width, heads * value_piece)
    outgate_cols = w_outgate.reshape(width, heads * value_piece)
    normed = rms_scale(tokens.astype(jnp.float32), norm_gain).astype(jnp.bfloat16)
    piece = lax.all_gather(normed, "ep", axis=0, tiled=True)
    projected = jnp.concatenate(
        [
            product(piece, query_cols),
            product(piece, key_cols),
            product(piece, value_cols),
            product(piece, outgate_cols),
        ],
        axis=1,
    ).astype(jnp.bfloat16)
    all_rows = projected.shape[0]
    narrow = heads * key_piece
    broad = heads * value_piece
    query_part = projected[:, :narrow].reshape(all_rows, heads, key_piece)
    key_part = projected[:, narrow : 2 * narrow].reshape(all_rows, heads, key_piece)
    value_part = projected[:, 2 * narrow : 2 * narrow + broad].reshape(all_rows, heads, value_piece)
    outgate_part = projected[:, 2 * narrow + broad :].reshape(all_rows, heads, value_piece)
    query, key, value, outgate = (
        lax.all_to_all(query_part, "ep", split_axis=0, concat_axis=2, tiled=True),
        lax.all_to_all(key_part, "ep", split_axis=0, concat_axis=2, tiled=True),
        lax.all_to_all(value_part, "ep", split_axis=0, concat_axis=2, tiled=True),
        lax.all_to_all(outgate_part, "ep", split_axis=0, concat_axis=2, tiled=True),
    )
    in_pre = product(normed, w_input)
    log_forget = jax.nn.log_sigmoid(product(normed, w_forget) + forget_bias)
    scaled = query.astype(jnp.float32) * key_size ** (-0.5)
    key_heads = key.astype(jnp.float32)
    value_heads = value.astype(jnp.float32)
    stab_next = jnp.maximum(log_forget + stabilizer, in_pre)
    decay = jnp.exp(log_forget + stabilizer - stab_next)
    inweight = jnp.exp(in_pre - stab_next)
    memory_next = decay[:, :, None, None] * memory + inweight[:, :, None, None] * (
        key_heads[:, :, :, None] * value_heads[:, :, None, :]
    )
    normalizer_next = decay[:, :, None] * normalizer + inweight[:, :, None] * key_heads
    numerator = jnp.einsum("shd,shde->she", scaled, memory_next, precision=lax.Precision.HIGHEST)
    denominator = jnp.sum(scaled * normalizer_next, axis=-1)
    hidden = numerator / jnp.maximum(jnp.abs(denominator), jnp.exp(-stab_next))[:, :, None]
    hidden = (
        hidden.reshape(seqs, value_width)
        * jax.nn.sigmoid(outgate.reshape(seqs, value_width).astype(jnp.float32))
    ).astype(jnp.bfloat16)
    partial_value = product(lax.all_gather(hidden, "ep", axis=0, tiled=True), w_out)
    summed = lax.psum(rounded_term(partial_value).astype(jnp.bfloat16), "tp")
    mixed = lax.all_to_all(summed, "ep", split_axis=0, concat_axis=1, tiled=True)
    resid = tokens.astype(jnp.float32) + mixed.astype(jnp.float32)
    ffn_in = rms_scale(resid, ffn_gain).astype(jnp.bfloat16)
    gate_local, up_local, down_local = (w_gate[0], w_up[0], w_down[0])
    n_experts = lax.axis_size("ep") * w_gate.shape[0]
    piece = lax.all_gather(ffn_in, "ep", axis=0, tiled=True)
    gate_part = product(piece, gate_local)
    up_part = product(piece, up_local)
    act = (jax.nn.silu(gate_part) * up_part).astype(jnp.bfloat16)
    expert_terms = rounded_term(product(act, down_local))
    labels = jnp.arange(n_experts, dtype=jnp.int32)
    route_dense = jnp.sum(
        jnp.where(expert_ids[:, :, None] == labels[None, None, :], route_weights[:, :, None], 0.0),
        axis=1,
    )
    my_weight = lax.all_to_all(route_dense, "ep", split_axis=1, concat_axis=0, tiled=True)
    contrib = expert_terms * my_weight
    n_ep = lax.axis_size("ep")
    n_tp = lax.axis_size("tp")
    arranged = jnp.swapaxes(contrib.reshape(n_ep, seqs, n_tp, width // n_tp), 1, 2)
    arranged = arranged.reshape(n_ep * n_tp * seqs, width // n_tp)
    mine = lax.psum_scatter(arranged, ("ep", "tp"), scatter_dimension=0, tiled=True)
    ffn_out = lax.all_gather(mine.astype(jnp.bfloat16), "tp", axis=1, tiled=True).astype(mine.dtype)
    out = (resid + ffn_out).astype(jnp.bfloat16)
    return (out, memory_next, normalizer_next, stab_next)


def solution(mesh):
    return jax.shard_map(
        body,
        mesh=mesh,
        in_specs=(
            P("ep", None),
            P("ep", "tp", None, None),
            P("ep", "tp", None),
            P("ep", "tp"),
            P(),
            P(None, "tp", "ep"),
            P(None, "tp", "ep"),
            P(None, "tp", "ep"),
            P(None, "tp", "ep"),
            P(None, "tp"),
            P(None, "tp"),
            P("tp"),
            P("tp", "ep"),
            P(),
            P("ep", None, "tp"),
            P("ep", None, "tp"),
            P("ep", "tp", None),
            P("ep", None),
            P("ep", None),
        ),
        out_specs=(P("ep", None), P("ep", "tp", None, None), P("ep", "tp", None), P("ep", "tp")),
        check_vma=False,
    )
```

profile of v0, /device:TPU:1, one launch (start us, length us, event | category | flops | bytes accessed | tf_op | source)
XLA Modules:
  0.0 273.7 jit_solution(16929384175384432204)
XLA Ops:
  0.7 1.1 fusion.14
  2.6 37.8 %all-gather = bf16[16,4,4096]{2,1,0:T(4,128)(2,1)S(1)} all-gather(bf16[1,4,4096]{2,1,0:T(4,128)(2,1)S(1)} %fusion.49), channel_id=1, replica_groups=mesh['ep'=16,'tp'=2] {'ep'}, dimensions={0}, use_global_device_ids=true | all-gather | bytes 557056 | tf_op jit(solution)/shard_map/all_gather | solution.py:50
  40.5 1.3 convolution_convert_fusion.4
  42.8 3.5 %all-to-all-start.1 = ((bf16[16,2,128]{2,1,0:T(2,128)(2,1)}), bf16[16,2,128]{2,1,0:T(2,128)(2,1)S(1)}, u32[]{:S(2)}, u32[]{:S(2)}) async-start(bf16[16,2,128]{2,1,0:T(2,128)(2,1)} %reshape.153), calls=%async_computation.1 | async-start | bytes 16384 | tf_op jit(solution)/shard_map/all_to_all | solution.py:69
  47.1 0.9 fusion.29
  48.0 0.9 subtract_exponential_fusion.1
  49.0 1.3 convolution_convert_fusion.5
  50.3 1.7 convolution_convert_fusion.3
  52.0 1.7 convolution_convert_fusion.2
  58.1 6.3 %all-to-all-start = ((bf16[16,2,128]{2,1,0:T(2,128)(2,1)}), bf16[16,2,128]{2,1,0:T(2,128)(2,1)S(1)}, u32[]{:S(2)}, u32[]{:S(2)}) async-start(bf16[16,2,128]{2,1,0:T(2,128)(2,1)} %reshape.149), calls=%async_computation | async-start | bytes 16384 | tf_op jit(solution)/shard_map/all_to_all | solution.py:68
  64.7 5.8 %all-to-all-done = bf16[16,2,128]{2,1,0:T(2,128)(2,1)S(1)} async-done(((bf16[16,2,128]{2,1,0:T(2,128)(2,1)}), bf16[16,2,128]{2,1,0:T(2,128)(2,1)S(1)}, u32[]{:S(2)}, u32[]{:S(2)}) %all-to-all-start) | async-done | bytes 8224 | tf_op jit(solution)/shard_map/all_to_all | solution.py:68
  70.5 3.5 %all-to-all-start.2 = ((bf16[16,2,256]{2,1,0:T(2,128)(2,1)}), bf16[16,2,256]{2,1,0:T(2,128)(2,1)S(1)}, u32[]{:S(2)}, u32[]{:S(2)}) async-start(bf16[16,2,256]{2,1,0:T(2,128)(2,1)} %reshape.151), calls=%async_computation.2 | async-start | bytes 32768 | tf_op jit(solution)/shard_map/all_to_all | solution.py:70
  75.2 4.9 %all-to-all-done.2 = bf16[16,2,256]{2,1,0:T(2,128)(2,1)S(1)} async-done(((bf16[16,2,256]{2,1,0:T(2,128)(2,1)}), bf16[16,2,256]{2,1,0:T(2,128)(2,1)S(1)}, u32[]{:S(2)}, u32[]{:S(2)}) %all-to-all-start.2) | async-done | bytes 16416 | tf_op jit(solution)/shard_map/all_to_all | solution.py:70
  80.1 3.5 %all-to-all-start.3 = ((bf16[16,2,256]{2,1,0:T(2,128)(2,1)}), bf16[16,2,256]{2,1,0:T(2,128)(2,1)S(1)}, u32[]{:S(2)}, u32[]{:S(2)}) async-start(bf16[16,2,256]{2,1,0:T(2,128)(2,1)} %reshape.155), calls=%async_computation.3 | async-start | bytes 32768 | tf_op jit(solution)/shard_map/all_to_all | solution.py:71
  83.9 4.2 %multiply_add_fusion = f32[4,4,256,512]{3,2,1,0:T(8,128)S(1)} fusion(f32[4,4,256,512]{3,2,1,0:T(8,128)} %param.20, f32[4,4,512]{2,1,0:T(4,128)S(1)} %reshape.121, f32[4,4,256]{2,1,0:T(4,128)S(1)} %reshape.120, f32[4,4]{1,0:T(4,128)S(1)} %subtract_exponential_fusion, f32[4,4]{1,0:T(4,128)S(1)} %get-tuple-element.6), kind=kLoop, calls=%fused_computation | loop fusion | flops 8388608 | bytes 16826496 | tf_op jit(solution)/shard_map/add | solution.py:81
  88.1 3.4 %copy-done.1 = f32[4,4,256,512]{3,2,1,0:T(8,128)} copy-done((f32[4,4,256,512]{3,2,1,0:T(8,128)}, f32[4,4,256,512]{3,2,1,0:T(8,128)S(1)}, u32[]{:S(2)}) %copy-start.1) | copy-done | bytes 8388632
  91.5 4.0 %fusion.30 = f32[4,4,1,512]{3,2,1,0:T(1,128)S(1)} fusion(f32[4,4,256,1]{2,3,1,0:T(1,128)S(1)} %reshape.141, f32[4,4,256,512]{3,2,1,0:T(8,128)S(1)} %multiply_add_fusion), kind=kOutput, calls=%fused_computation.57 | convolution fusion | flops 25165824 | bytes 8437760 | tf_op jit(solution)/shard_map/shd,shde->she/dot_general | solution.py:85
  95.6 6.3 %all-to-all-start.5 = ((f32[4,16,1]{0,2,1:T(1,128)}), f32[4,16,1]{0,2,1:T(1,128)S(1)}, u32[]{:S(2)}, u32[]{:S(2)}) async-start(f32[4,16,1]{0,2,1:T(1,128)} %copy.131), calls=%async_computation.5 | async-start | bytes 16384 | tf_op jit(solution)/shard_map/all_to_all | solution.py:109
  102.5 34.9 %all-gather.1 = bf16[16,4,2048]{2,1,0:T(4,128)(2,1)S(1)} all-gather(bf16[1,4,2048]{2,1,0:T(4,128)(2,1)S(1)} %fusion.25), channel_id=1, replica_groups=mesh['ep'=16,'tp'=2] {'ep'}, dimensions={0}, use_global_device_ids=true | all-gather | bytes 278528 | tf_op jit(solution)/shard_map/all_gather | solution.py:92
  138.1 1.2 convolution_convert_fusion.1
  139.4 22.3 %psum.7 = bf16[16,4,256]{2,1,0:T(4,128)(2,1)} all-reduce(bf16[16,4,256]{2,1,0:T(4,128)(2,1)S(1)} %all_to_all.24), channel_id=1, replica_groups=mesh['ep'=16,'tp'=2] {'tp'}, use_global_device_ids=true, to_apply=%region_2.3 | all-reduce | flops 16384 | bytes 65536 | tf_op jit(solution)/shard_map/psum | solution.py:93
  161.7 3.5 %all-to-all-start.4 = ((bf16[16,4,256]{2,1,0:T(4,128)(2,1)}), bf16[16,4,256]{2,1,0:T(4,128)(2,1)S(1)}, u32[]{:S(2)}, u32[]{:S(2)}) async-start(bf16[16,4,256]{2,1,0:T(4,128)(2,1)} %psum.7), calls=%async_computation.4 | async-start | bytes 65536 | tf_op jit(solution)/shard_map/all_to_all | solution.py:94
  165.4 6.1 %all-to-all-done.4 = bf16[16,4,256]{2,1,0:T(4,128)(2,1)S(1)} async-done(((bf16[16,4,256]{2,1,0:T(4,128)(2,1)}), bf16[16,4,256]{2,1,0:T(4,128)(2,1)S(1)}, u32[]{:S(2)}, u32[]{:S(2)}) %all-to-all-start.4) | async-done | bytes 32800 | tf_op jit(solution)/shard_map/all_to_all | solution.py:94
  171.7 32.5 %all-gather.2 = bf16[16,4,4096]{2,1,0:T(4,128)(2,1)S(1)} all-gather(bf16[1,4,4096]{2,1,0:T(4,128)(2,1)S(1)} %fusion.22), channel_id=1, replica_groups=mesh['ep'=16,'tp'=2] {'ep'}, dimensions={0}, use_global_device_ids=true | all-gather | bytes 557056 | tf_op jit(solution)/shard_map/all_gather | solution.py:99
  204.3 2.1 fusion.3
  206.4 3.8 %convolution_convert_fusion = bf16[64,4096]{1,0:T(8,128)(2,1)} fusion(bf16[1,256,4096]{2,1,0:T(8,128)(2,1)S(1)} %copy-done, bf16[64,4096]{1,0:T(8,128)(2,1)S(1)} %reshape.137, bf16[1,4096,256]{2,1,0:T(8,128)(2,1)} %param.34, f32[64,256]{1,0:T(8,128)S(1)} %fusion.3), kind=kOutput, calls=%fused_computation.1 | convolution fusion | flops 268795904 | bytes 5308416 | tf_op jit(solution)/shard_map/dot_general | solution.py:12
  210.2 1.2 convert_multiply_fusion
  211.3 1.9 reshape.118
  213.2 1.9 copy.132
  215.1 1.3 reshape.119
  216.5 53.1 %all-reduce.2 = bf16[128,2048]{1,0:T(8,128)(2,1)S(1)} all-reduce(f32[128,2048]{1,0:T(8,128)} %reshape.119), channel_id=2, replica_groups=mesh['ep'=16,'tp'=2] {'ep','tp'}, use_global_device_ids=true, to_apply=%region_5.6.clone | all-reduce | flops 262144 | bytes 1572864
  269.7 3.4 %all_gather.15 = bf16[4,4096]{1,0:T(4,128)(2,1)S(1)} all-gather(bf16[4,2048]{1,0:T(4,128)(2,1)S(1)} %dynamic-slice_convert_fusion), channel_id=1, replica_groups=mesh['ep'=16,'tp'=2] {'tp'}, dimensions={1}, use_global_device_ids=true | all-gather | bytes 49152 | tf_op jit(solution)/shard_map/all_gather | solution.py:116
  (74 shorter events, 11.3 us)
Async XLA Ops:
  0.6 205.7 %copy-start = (bf16[1,256,4096]{2,1,0:T(8,128)(2,1)S(1)}, bf16[1,256,4096]{2,1,0:T(8,128)(2,1)}, u32[]{:S(2)}) copy-start(bf16[1,256,4096]{2,1,0:T(8,128)(2,1)} %param.35) | copy-start | bytes 6291460
  0.6 73.8 %copy-start.5 = (f32[4,4,256]{2,1,0:T(4,128)S(1)}, f32[4,4,256]{2,1,0:T(4,128)}, u32[]{:S(2)}) copy-start(f32[4,4,256]{2,1,0:T(4,128)} %param.21) | copy-start | bytes 49156
  42.8 15.3 %all-to-all-start.1 = ((bf16[16,2,128]{2,1,0:T(2,128)(2,1)}), bf16[16,2,128]{2,1,0:T(2,128)(2,1)S(1)}, u32[]{:S(2)}, u32[]{:S(2)}) async-start(bf16[16,2,128]{2,1,0:T(2,128)(2,1)} %reshape.153), calls=%async_computation.1 | async-start | bytes 16384 | tf_op jit(solution)/shard_map/all_to_all | solution.py:69
  49.0 39.1 %copy-start.6 = (f32[4,4]{1,0:T(4,128)}, f32[4,4]{1,0:T(4,128)S(1)}, u32[]{:S(2)}) copy-start(f32[4,4]{1,0:T(4,128)S(1)} %get-tuple-element.7) | copy-start | bytes 196
  58.1 12.4 %all-to-all-start = ((bf16[16,2,128]{2,1,0:T(2,128)(2,1)}), bf16[16,2,128]{2,1,0:T(2,128)(2,1)S(1)}, u32[]{:S(2)}, u32[]{:S(2)}) async-start(bf16[16,2,128]{2,1,0:T(2,128)(2,1)} %reshape.149), calls=%async_computation | async-start | bytes 16384 | tf_op jit(solution)/shard_map/all_to_all | solution.py:68
  70.5 9.7 %all-to-all-start.2 = ((bf16[16,2,256]{2,1,0:T(2,128)(2,1)}), bf16[16,2,256]{2,1,0:T(2,128)(2,1)S(1)}, u32[]{:S(2)}, u32[]{:S(2)}) async-start(bf16[16,2,256]{2,1,0:T(2,128)(2,1)} %reshape.151), calls=%async_computation.2 | async-start | bytes 32768 | tf_op jit(solution)/shard_map/all_to_all | solution.py:70
  80.1 15.5 %all-to-all-start.3 = ((bf16[16,2,256]{2,1,0:T(2,128)(2,1)}), bf16[16,2,256]{2,1,0:T(2,128)(2,1)S(1)}, u32[]{:S(2)}, u32[]{:S(2)}) async-start(bf16[16,2,256]{2,1,0:T(2,128)(2,1)} %reshape.155), calls=%async_computation.3 | async-start | bytes 32768 | tf_op jit(solution)/shard_map/all_to_all | solution.py:71
  88.1 3.4 %copy-start.1 = (f32[4,4,256,512]{3,2,1,0:T(8,128)}, f32[4,4,256,512]{3,2,1,0:T(8,128)S(1)}, u32[]{:S(2)}) copy-start(f32[4,4,256,512]{3,2,1,0:T(8,128)S(1)} %multiply_add_fusion) | copy-start | bytes 25165828
  91.5 46.7 %copy-start.3 = (bf16[2048,256]{1,0:T(8,128)(2,1)S(1)}, bf16[2048,256]{1,0:T(8,128)(2,1)}, u32[]{:S(2)}) copy-start(bf16[2048,256]{1,0:T(8,128)(2,1)} %param.31) | copy-start | bytes 3145732
  91.5 80.0 %copy-start.2 = (bf16[4,4096]{1,0:T(4,128)(2,1)S(1)}, bf16[4,4096]{1,0:T(4,128)(2,1)}, u32[]{:S(2)}) copy-start(bf16[4,4096]{1,0:T(4,128)(2,1)} %param.19) | copy-start | bytes 98308
  91.5 80.2 %copy-start.4 = (f32[4096]{0:T(1024)S(1)}, f32[4096]{0:T(1024)}, u32[]{:S(2)}) copy-start(f32[4096]{0:T(1024)} %param.32) | copy-start | bytes 49156
  95.6 66.1 %all-to-all-start.5 = ((f32[4,16,1]{0,2,1:T(1,128)}), f32[4,16,1]{0,2,1:T(1,128)S(1)}, u32[]{:S(2)}, u32[]{:S(2)}) async-start(f32[4,16,1]{0,2,1:T(1,128)} %copy.131), calls=%async_computation.5 | async-start | bytes 16384 | tf_op jit(solution)/shard_map/all_to_all | solution.py:109
  161.7 9.7 %all-to-all-start.4 = ((bf16[16,4,256]{2,1,0:T(4,128)(2,1)}), bf16[16,4,256]{2,1,0:T(4,128)(2,1)S(1)}, u32[]{:S(2)}, u32[]{:S(2)}) async-start(bf16[16,4,256]{2,1,0:T(4,128)(2,1)} %psum.7), calls=%async_computation.4 | async-start | bytes 65536 | tf_op jit(solution)/shard_map/all_to_all | solution.py:94
where the time goes:
time: 275 us; the launch traced here: 274 us
  blocking collectives  184 us (67%)
  starting transfers between devices  26.6 us (10%)
  matrix products  19 us (7%)
  waiting for transfers between devices  16.8 us (6%)
  local copies, waits for them, and re-layouts  15.6 us (6%)
  other arithmetic  10.7 us (4%)
    unnamed x1, blocking collectives  53.1 us
    all_gather x1, blocking collectives, body(): piece = lax.all_gather(normed, 'ep', axis=0, tiled=True)  37.8 us
    all_gather x1, blocking collectives, body(): lax.all_gather(hidden, 'ep', axis=0, tiled=True)  34.9 us
    all_gather x1, blocking collectives, body(): piece = lax.all_gather(ffn_in, 'ep', axis=0, tiled=True)  32.5 us
    psum x1, blocking collectives, body(): summed = lax.psum(rounded_term(partial_value).astype(jnp.bfloat16), 'tp')  22.3 us
    dot_general x9, matrix products, product(): return jnp.dot(left, right, preferred_element_type=jnp.float32)  15 us
    unnamed x26, local copies, waits for them, and re-layouts  7.67 us
    all_to_all x1, starting transfers between devices, body(): lax.all_to_all(route_dense, 'ep', split_axis=1, concat_axis=0, tiled=True)  6.33 us
  transfers between devices with their start and end apart: 6, of which 3 were waited for; matrix products, arithmetic and copies ran while one was open for 9% of the time, Pallas kernels for 0%

commit v1 on v0

v1 whole, which is shorter than its diff:
```python
import functools

import jax
import jax.numpy as jnp
from jax import lax
from jax.experimental import pallas as pl
from jax.experimental.pallas import tpu as pltpu
from jax.sharding import PartitionSpec as P

MESH = pl.DeviceIdType.MESH
VMEM_LIMIT = 48 * 1024 * 1024


def product(left, right):
    return jnp.dot(left, right, preferred_element_type=jnp.float32)


def product_nt(left, right):
    return lax.dot_general(left, right, (((1,), (1,)), ((), ())), preferred_element_type=jnp.float32)


def rms_scale(values, gain):
    return values * lax.rsqrt(jnp.mean(values * values, axis=-1, keepdims=True) + 1e-06) * gain


def remote(src, dst, send_sem, recv_sem, device):
    return pltpu.make_async_remote_copy(
        src_ref=src, dst_ref=dst, send_sem=send_sem, recv_sem=recv_sem, device_id=device, device_id_type=MESH
    )


def each(low, high, step):
    def run(at, carry):
        step(at)
        return carry

    lax.fori_loop(low, high, run, 0)


def stack_rows(pieces, dest):
    rows = pieces[0]().shape[0]
    group = max(1, 16 // rows)
    for first in range(0, len(pieces), group):
        block = jnp.concatenate([piece() for piece in pieces[first : first + group]], axis=0)
        dest[first * rows : first * rows + block.shape[0], :] = block.astype(jnp.bfloat16)


class HalfGather:
    def __init__(self, n, own, gathered, sems):
        self.n, self.own, self.gathered = n, own, gathered
        self.send, self.recv, self.relay_send, self.relay_recv = sems
        self.me, self.t = lax.axis_index("ep"), lax.axis_index("tp")

    def source(self, d):
        return lax.rem(self.me + self.n - d, self.n)

    def out(self, d):
        return remote(
            self.own.at[self.t],
            self.gathered.at[self.me, self.t],
            self.send.at[d],
            self.recv.at[d],
            (lax.rem(self.me + d, self.n), self.t),
        )

    def arrival(self, d):
        slot = self.gathered.at[self.source(d), self.t]
        return remote(self.own.at[self.t], slot, self.send.at[d], self.recv.at[d], (self.me, 1 - self.t))

    def relay(self, d, half):
        slot = self.gathered.at[self.source(d), half]
        return remote(slot, slot, self.relay_send.at[d], self.relay_recv.at[d], (self.me, 1 - self.t))

    def start(self):
        each(1, self.n, lambda d: self.out(d).start())
        self.gathered[self.me] = self.own[...]

    def finish(self):
        def pass_on(d):
            self.arrival(d).wait_recv()
            self.relay(d, self.t).start()

        each(1, self.n, pass_on)
        each(1, self.n, lambda d: self.relay(d, 1 - self.t).wait_recv())

    def drain(self):
        def step(d):
            self.out(d).wait_send()
            self.relay(d, self.t).wait_send()

        each(1, self.n, step)


class Exchange:
    def __init__(self, n, outbox, inbox, send, recv, broadcast=False):
        self.n, self.outbox, self.inbox, self.send, self.recv = n, outbox, inbox, send, recv
        self.broadcast = broadcast
        self.me, self.t = lax.axis_index("ep"), lax.axis_index("tp")

    def out(self, d):
        to = lax.rem(self.me + d, self.n)
        src = self.outbox if self.broadcast else self.outbox.at[to]
        return remote(src, self.inbox.at[self.me], self.send.at[d], self.recv.at[d], (to, self.t))

    def arrival(self, d):
        source = lax.rem(self.me + self.n - d, self.n)
        src = self.outbox if self.broadcast else self.outbox.at[source]
        return remote(src, self.inbox.at[source], self.send.at[d], self.recv.at[d], (source, self.t))

    def start(self):
        each(1, self.n, lambda d: self.out(d).start())
        self.inbox[self.me] = self.outbox[...] if self.broadcast else self.outbox[self.me]

    def finish(self):
        each(1, self.n, lambda d: self.arrival(d).wait_recv())

    def drain(self):
        each(1, self.n, lambda d: self.out(d).wait_send())


def cell_in_kernel(
    n,
    tokens_ref, gain_ref, win_ref, wforget_ref, wq_ref, wk_ref, wv_ref, wo_ref,
    inpre_ref, fpre_ref, proj_ref,
    own, gathered, weights, rows_lo, rows_hi, outbox, inbox,
    wsem, send, recv, rsend, rrecv, xsend, xrecv,
):
    me, t = lax.axis_index("ep"), lax.axis_index("tp")
    loads, first = [], 0
    for index, ref in enumerate((wq_ref, wk_ref, wv_ref, wo_ref)):
        count = ref.shape[0]
        loads.append(pltpu.make_async_copy(ref, weights.at[pl.ds(first, count)], wsem.at[index]))
        first += count
    for load in loads:
        load.start()
    barrier = pltpu.get_barrier_semaphore()
    each(1, n, lambda d: pl.semaphore_signal(barrier, inc=1, device_id=(lax.rem(me + d, n), t), device_id_type=MESH))
    pl.semaphore_signal(barrier, inc=1, device_id=(me, 1 - t), device_id_type=MESH)

    half = own.shape[2]
    seqs = own.shape[1]
    normed = rms_scale(tokens_ref[...].astype(jnp.float32), gain_ref[...]).astype(jnp.bfloat16)
    own[0] = normed[:, :half]
    own[1] = normed[:, half:]
    pl.semaphore_wait(barrier, n)

    gather = HalfGather(n, own, gathered, (send, recv, rsend, rrecv))
    gather.start()
    inpre_ref[...] = product_nt(normed, win_ref[...])
    fpre_ref[...] = product_nt(normed, wforget_ref[...])
    gather.finish()
    for index, dest in enumerate((rows_lo, rows_hi)):
        stack_rows([functools.partial(lambda p, i: gathered[p, i].astype(jnp.float32), p, index) for p in range(n)], dest)
    for load in loads:
        load.wait()
    result = product_nt(rows_lo[...], weights[:, :half]) + product_nt(rows_hi[...], weights[:, half:])
    for p in range(n):
        outbox[p] = result[p * seqs : (p + 1) * seqs].astype(jnp.bfloat16)
    swap = Exchange(n, outbox, inbox, xsend, xrecv)
    swap.start()
    swap.finish()
    proj_ref[...] = inbox[...]
    gather.drain()
    swap.drain()


def ffn_kernel(
    n,
    hidden_ref, tokens_ref, gain_ref, route_ref, wout_ref, wgate_ref, wup_ref, wdown_ref,
    out_ref,
    heads_in, rows_h, wout, mixbox, mixin, resid, own, gathered, rows_lo, rows_hi,
    wgate, wup, wdown, terms, other, outbox, inbox, halves,
    wsem, hsend, hrecv, msend, mrecv, send, recv, rsend, rrecv, tsend, trecv, xsend, xrecv, osend, orecv,
):
    me, t = lax.axis_index("ep"), lax.axis_index("tp")
    loads = [
        pltpu.make_async_copy(ref, dest, wsem.at[index])
        for index, (ref, dest) in enumerate(((wout_ref, wout), (wgate_ref, wgate), (wup_ref, wup), (wdown_ref, wdown)))
    ]
    for load in loads:
        load.start()
    barrier = pltpu.get_barrier_semaphore()

    def greet(d):
        to = lax.rem(me + d, n)
        pl.semaphore_signal(barrier, inc=1, device_id=(to, t), device_id_type=MESH)
        pl.semaphore_signal(barrier, inc=1, device_id=(to, 1 - t), device_id_type=MESH)

    each(1, n, greet)
    pl.semaphore_signal(barrier, inc=1, device_id=(me, 1 - t), device_id_type=MESH)
    pl.semaphore_wait(barrier, 2 * n - 1)

    seqs, half = own.shape[1], own.shape[2]
    heads = Exchange(n, hidden_ref, heads_in, hsend, hrecv, broadcast=True)
    heads.start()
    heads.finish()
    stack_rows([functools.partial(lambda p: heads_in[p].astype(jnp.float32), p) for p in range(n)], rows_h)
    loads[0].wait()
    partial_value = product(rows_h[...], wout[...])
    for p in range(n):
        mixbox[p] = partial_value[p * seqs : (p + 1) * seqs].astype(jnp.bfloat16)

    def mix_out(d, c):
        to = lax.rem(me + d, n)
        to_t = t if c == 0 else 1 - t
        return remote(mixbox.at[to], mixin.at[t, me], msend.at[c, d], mrecv.at[c, d], (to, to_t))

    def mix_arrival(d, c):
        source = lax.rem(me + n - d, n)
        from_t = t if c == 0 else 1 - t
        return remote(mixbox.at[source], mixin.at[from_t, source], msend.at[c, d], mrecv.at[c, d], (source, 1 - t))

    each(1, n, lambda d: mix_out(d, 0).start())
    each(0, n, lambda d: mix_out(d, 1).start())
    mixin[t, me] = mixbox[me]
    each(1, n, lambda d: mix_arrival(d, 0).wait_recv())
    each(0, n, lambda d: mix_arrival(d, 1).wait_recv())
    piece = mixin.shape[3]
    for p in range(n):
        mixed = (mixin[0, p].astype(jnp.float32) + mixin[1, p].astype(jnp.float32)).astype(jnp.bfloat16)
        columns = slice(p * piece, (p + 1) * piece)
        resid[:, columns] = tokens_ref[:, columns].astype(jnp.float32) + mixed.astype(jnp.float32)
    ffn_in = rms_scale(resid[...], gain_ref[...]).astype(jnp.bfloat16)
    own[0] = ffn_in[:, :half]
    own[1] = ffn_in[:, half:]
    gather = HalfGather(n, own, gathered, (send, recv, rsend, rrecv))
    gather.start()
    gather.finish()
    for index, dest in enumerate((rows_lo, rows_hi)):
        stack_rows([functools.partial(lambda p, i: gathered[p, i].astype(jnp.float32), p, index) for p in range(n)], dest)
    loads[1].wait()
    gate = product(rows_lo[...], wgate[:half]) + product(rows_hi[...], wgate[half:])
    loads[2].wait()
    up = product(rows_lo[...], wup[:half]) + product(rows_hi[...], wup[half:])
    act = (jax.nn.silu(gate) * up).astype(jnp.bfloat16)
    loads[3].wait()
    width = min(512, half)
    for index in range(2):
        for first in range(0, half, width):
            block = product(act, wdown[:, index * half + first : index * half + first + width])
            terms[index, :, first : first + width] = block.astype(jnp.bfloat16)
    across = remote(terms.at[1 - t], other, tsend, trecv, (me, 1 - t))
    across.start()
    across.wait_recv()
    rows = max(seqs, 16)
    for first in range(0, n * seqs, rows):
        both = terms[t, first : first + rows].astype(jnp.float32) + other[first : first + rows].astype(jnp.float32)
        for at in range(rows // seqs):
            outbox[first // seqs + at] = both[at * seqs : (at + 1) * seqs].astype(jnp.bfloat16)
    swap = Exchange(n, outbox, inbox, xsend, xrecv)
    swap.start()
    swap.finish()
    total = route_ref[:, 0:1] * inbox[0].astype(jnp.float32)
    for p in range(1, n):
        total = total + route_ref[:, p : p + 1] * inbox[p].astype(jnp.float32)
    halves[t] = total.astype(jnp.bfloat16)
    give = remote(halves.at[t], halves.at[t], osend, orecv, (me, 1 - t))
    take = remote(halves.at[1 - t], halves.at[1 - t], osend, orecv, (me, 1 - t))
    give.start()
    take.wait_recv()
    for index in range(2):
        columns = slice(index * half, (index + 1) * half)
        out_ref[:, columns] = (resid[:, columns] + halves[index].astype(jnp.float32)).astype(jnp.bfloat16)
    heads.drain()
    each(1, n, lambda d: mix_out(d, 0).wait_send())
    each(0, n, lambda d: mix_out(d, 1).wait_send())
    gather.drain()
    across.wait_send()
    swap.drain()
    give.wait_send()


def vmem_spec():
    return pl.BlockSpec(memory_space=pltpu.VMEM)


def any_spec():
    return pl.BlockSpec(memory_space=pl.ANY)


def cell_in(n, tokens, gain, w_input, w_forget, w_query, w_key, w_value, w_outgate):
    seqs, width = tokens.shape
    flat = [jnp.transpose(w, (1, 2, 0)).reshape(-1, width) for w in (w_query, w_key, w_value, w_outgate)]
    columns = sum(w.shape[0] for w in flat)
    heads = w_input.shape[1]
    bf16 = jnp.bfloat16
    dma = pltpu.SemaphoreType.DMA
    return pl.pallas_call(
        functools.partial(cell_in_kernel, n),
        out_shape=(
            jax.ShapeDtypeStruct((seqs, heads), jnp.float32),
            jax.ShapeDtypeStruct((seqs, heads), jnp.float32),
            jax.ShapeDtypeStruct((n, seqs, columns), bf16),
        ),
        in_specs=[vmem_spec()] * 4 + [any_spec()] * 4,
        out_specs=(vmem_spec(),) * 3,
        scratch_shapes=[
            pltpu.VMEM((2, seqs, width // 2), bf16),
            pltpu.VMEM((n, 2, seqs, width // 2), bf16),
            pltpu.VMEM((columns, width), bf16),
            pltpu.VMEM((n * seqs, width // 2), bf16),
            pltpu.VMEM((n * seqs, width // 2), bf16),
            pltpu.VMEM((n, seqs, columns), bf16),
            pltpu.VMEM((n, seqs, columns), bf16),
            dma((4,)),
        ]
        + [dma((n,))] * 6,
        compiler_params=pltpu.CompilerParams(collective_id=0, has_side_effects=True, vmem_limit_bytes=VMEM_LIMIT),
        name="cell_in",
    )(tokens, gain.reshape(1, width), w_input.T, w_forget.T, *flat)


def ffn(n, hidden, tokens, gain, route, w_out, w_gate, w_up, w_down):
    seqs, width = tokens.shape
    half = width // 2
    bf16 = jnp.bfloat16
    dma = pltpu.SemaphoreType.DMA
    return pl.pallas_call(
        functools.partial(ffn_kernel, n),
        out_shape=jax.ShapeDtypeStruct((seqs, width), bf16),
        in_specs=[vmem_spec()] * 4 + [any_spec()] * 4,
        out_specs=vmem_spec(),
        scratch_shapes=[
            pltpu.VMEM((n, seqs, hidden.shape[1]), bf16),
            pltpu.VMEM((n * seqs, hidden.shape[1]), bf16),
            pltpu.VMEM(w_out.shape, bf16),
            pltpu.VMEM((n, seqs, w_out.shape[1]), bf16),
            pltpu.VMEM((2, n, seqs, w_out.shape[1]), bf16),
            pltpu.VMEM((seqs, width), jnp.float32),
            pltpu.VMEM((2, seqs, half), bf16),
            pltpu.VMEM((n, 2, seqs, half), bf16),
            pltpu.VMEM((n * seqs, half), bf16),
            pltpu.VMEM((n * seqs, half), bf16),
            pltpu.VMEM(w_gate.shape, bf16),
            pltpu.VMEM(w_up.shape, bf16),
            pltpu.VMEM(w_down.shape, bf16),
            pltpu.VMEM((2, n * seqs, half), bf16),
            pltpu.VMEM((n * seqs, half), bf16),
            pltpu.VMEM((n, seqs, half), bf16),
            pltpu.VMEM((n, seqs, half), bf16),
            pltpu.VMEM((2, seqs, half), bf16),
            dma((4,)),
            dma((n,)),
            dma((n,)),
            dma((2, n)),
            dma((2, n)),
            dma((n,)),
            dma((n,)),
            dma((n,)),
            dma((n,)),
            dma,
            dma,
            dma((n,)),
            dma((n,)),
            dma,
            dma,
        ],
        compiler_params=pltpu.CompilerParams(collective_id=1, has_side_effects=True, vmem_limit_bytes=VMEM_LIMIT),
        name="ffn",
    )(hidden, tokens, gain.reshape(1, width), route, w_out, w_gate, w_up, w_down)


def body(
    tokens,
    memory,
    normalizer,
    stabilizer,
    norm_gain,
    w_query,
    w_key,
    w_value,
    w_outgate,
    w_input,
    w_forget,
    forget_bias,
    w_out,
    ffn_gain,
    w_gate,
    w_up,
    w_down,
    expert_ids,
    route_weights,
):
    n = lax.axis_size("ep")
    seqs, width = tokens.shape
    heads, key_size, value_size = (memory.shape[1], memory.shape[2], memory.shape[3])
    value_width = heads * value_size
    key_piece = w_query.shape[2]
    value_piece = w_value.shape[2]
    in_pre, forget_pre, projected = cell_in(
        n, tokens, norm_gain, w_input, w_forget, w_query, w_key, w_value, w_outgate
    )
    narrow = heads * key_piece
    broad = heads * value_piece

    def split(first, piece):
        part = projected[:, :, first : first + heads * piece].reshape(n, seqs, heads, piece)
        return jnp.transpose(part, (1, 2, 0, 3)).reshape(seqs, heads, n * piece).astype(jnp.float32)

    query, key_heads = split(0, key_piece), split(narrow, key_piece)
    value_heads, outgate = split(2 * narrow, value_piece), split(2 * narrow + broad, value_piece)
    log_forget = jax.nn.log_sigmoid(forget_pre + forget_bias)
    scaled = query * key_size ** (-0.5)
    stab_next = jnp.maximum(log_forget + stabilizer, in_pre)
    decay = jnp.exp(log_forget + stabilizer - stab_next)
    inweight = jnp.exp(in_pre - stab_next)
    memory_next = decay[:, :, None, None] * memory + inweight[:, :, None, None] * (
        key_heads[:, :, :, None] * value_heads[:, :, None, :]
    )
    normalizer_next = decay[:, :, None] * normalizer + inweight[:, :, None] * key_heads
    numerator = jnp.einsum("shd,shde->she", scaled, memory_next, precision=lax.Precision.HIGHEST)
    denominator = jnp.sum(scaled * normalizer_next, axis=-1)
    hidden = numerator / jnp.maximum(jnp.abs(denominator), jnp.exp(-stab_next))[:, :, None]
    hidden = (hidden * jax.nn.sigmoid(outgate)).reshape(seqs, value_width).astype(jnp.bfloat16)
    labels = jnp.arange(n, dtype=jnp.int32)
    route = jnp.sum(
        jnp.where(expert_ids[:, :, None] == labels[None, None, :], route_weights[:, :, None], 0.0), axis=1
    )
    out = ffn(n, hidden, tokens, ffn_gain, route, w_out, w_gate[0], w_up[0], w_down[0])
    return (out, memory_next, normalizer_next, stab_next)


def solution(mesh):
    return jax.shard_map(
        body,
        mesh=mesh,
        in_specs=(
            P("ep", None),
            P("ep", "tp", None, None),
            P("ep", "tp", None),
            P("ep", "tp"),
            P(),
            P(None, "tp", "ep"),
            P(None, "tp", "ep"),
            P(None, "tp", "ep"),
            P(None, "tp", "ep"),
            P(None, "tp"),
            P(None, "tp"),
            P("tp"),
            P("tp", "ep"),
            P(),
            P("ep", None, "tp"),
            P("ep", None, "tp"),
            P("ep", "tp", None),
            P("ep", None),
            P("ep", None),
        ),
        out_specs=(P("ep", None), P("ep", "tp", None, None), P("ep", "tp", None), P("ep", "tp")),
        check_vma=False,
    )
```

time: 275 us -> 81.9 us (0.30)
  blocking collectives: 184 us -> 0 us
  Pallas kernels: 0 us -> 59.1 us
  starting transfers between devices: 26.6 us -> 0 us
  waiting for transfers between devices: 16.8 us -> 0 us
  matrix products: 19 us -> 4.05 us
  local copies, waits for them, and re-layouts: 15.6 us -> 10.6 us
  other arithmetic: 10.7 us -> 6.59 us
    all_gather x4 -> x0, blocking collectives: 109 us -> none  [the longest x1 37.8 us: body(): piece = lax.all_gather(normed, 'ep', axis=0, tiled=True)]
    pallas_call x0 -> x2, Pallas kernels: none -> 59.1 us  [the longest x1 37.3 us: ffn(): pl.pallas_call(functools.partial(ffn_kernel, n), out_shape=jax.ShapeDtype...]
    unnamed x1 -> x0, blocking collectives: 53.1 us -> none
    all_to_all x6 -> x0, starting transfers between devices: 26.6 us -> none  [the longest x1 6.33 us: body(): lax.all_to_all(route_dense, 'ep', split_axis=1, concat_axis=0, tiled=True)]
    psum x1 -> x0, blocking collectives: 22.3 us -> none  [body(): summed = lax.psum(rounded_term(partial_value).astype(jnp.bfloat16), 'tp')]
    all_to_all x6 -> x0, waiting for transfers between devices: 16.8 us -> none  [the longest x1 6.1 us: body(): lax.all_to_all(summed, 'ep', split_axis=0, concat_axis=1, tiled=True)]
    dot_general x9 -> x0, matrix products: 15 us -> none  [product(): return jnp.dot(left, right, preferred_element_type=jnp.float32)]
    reshape x6 -> x0, local copies, waits for them, and re-layouts: 3.71 us -> none  [the longest x1 1.88 us: body(): contrib.reshape(n_ep, seqs, n_tp, width // n_tp)]
  transfers between devices with their start and end apart: 6 -> 0, of which waited for: 3 -> 0; matrix products, arithmetic and copies ran while one was open for 9% -> 0% of each run, Pallas kernels for 0% -> 0%
where the time goes in v1:
time: 81.9 us; the launch traced here: 81.3 us
  Pallas kernels  59.1 us (72%)
  local copies, waits for them, and re-layouts  10.6 us (13%)
  other arithmetic  6.59 us (8%)
  matrix products  4.05 us (5%)
  between operations  0.89 us (1%)
    pallas_call x1, Pallas kernels, ffn(): pl.pallas_call(functools.partial(ffn_kernel, n), out_shape=jax.ShapeDtype...  37.3 us
    pallas_call x1, Pallas kernels, cell_in(): pl.pallas_call(functools.partial(cell_in_kernel, n), out_shape=(jax.Shape...  21.8 us
    unnamed x36, local copies, waits for them, and re-layouts  9.39 us
    add x1, other arithmetic, body(): decay[:, :, None, None] * memory  4.18 us
    dot_general x1, matrix products, body(): jnp.einsum('shd,shde->she', scaled, memory_next, precision=lax.Precision....  4.05 us

profile of v1, /device:TPU:1, one launch (start us, length us, event | category | flops | bytes accessed | tf_op | source)
XLA Modules:
  0.0 81.3 jit_solution(1996336376638897799)
XLA Ops:
  0.6 1.2 %copy-done.2 = bf16[4096,4,32]{0,2,1:T(8,128)(2,1)S(1)} copy-done((bf16[4096,4,32]{0,2,1:T(8,128)(2,1)S(1)}, bf16[4096,4,32]{0,2,1:T(8,128)(2,1)}, u32[]{:S(2)}) %copy-start.2) | copy-done | bytes 1048600
  1.9 1.2 %copy-done.3 = bf16[4096,4,32]{0,2,1:T(8,128)(2,1)S(1)} copy-done((bf16[4096,4,32]{0,2,1:T(8,128)(2,1)S(1)}, bf16[4096,4,32]{0,2,1:T(8,128)(2,1)}, u32[]{:S(2)}) %copy-start.3) | copy-done | bytes 1048600
  3.1 1.0 %copy-done.5 = bf16[4096,4,16]{0,2,1:T(8,128)(2,1)S(1)} copy-done((bf16[4096,4,16]{0,2,1:T(8,128)(2,1)S(1)}, bf16[4096,4,16]{0,2,1:T(8,128)(2,1)}, u32[]{:S(2)}) %copy-start.5) | copy-done | bytes 524312
  4.1 1.0 %copy-done.6 = bf16[4096,4,16]{0,2,1:T(8,128)(2,1)S(1)} copy-done((bf16[4096,4,16]{0,2,1:T(8,128)(2,1)S(1)}, bf16[4096,4,16]{0,2,1:T(8,128)(2,1)}, u32[]{:S(2)}) %copy-start.6) | copy-done | bytes 524312
  5.2 0.8 copy-done.7
  5.9 0.8 copy-done.9
  6.7 0.8 copy-done.10
  7.4 0.7 copy-done.11
  8.2 21.8 %cell_in.1 = (f32[4,4]{1,0:T(4,128)S(1)}, f32[4,4]{1,0:T(4,128)S(1)}, bf16[16,4,384]{2,1,0:T(4,128)(2,1)S(1)}) custom-call(bf16[4,4096]{1,0:T(4,128)(2,1)S(1)} %copy-done.7, f32[1,4096]{1,0:T(1,128)S(1)} %bitcast.55, bf16[4,4096]{1,0:T(4,128)(2,1)S(1)} %bitcast.53, bf16[4,4096]{1,0:T(4,128)(2,1)S(1)} %bitcast.54, bf16[64,4096]{1,0:T(8,128)(2,1)S(1)} %bitcast.50, ...), custom_call_target="tpu_custom_call" | custom-call | tf_op jit(solution)/shard_map/cell_in/pallas_call | solution.py:288
  30.0 0.1 reshape.91
  30.2 0.1 reshape.85
  30.3 0.7 subtract_exponential_fusion.1
  31.0 0.0 copy-start.14
  31.0 0.1 mul.68
  31.2 0.1 mul.70
  31.3 0.1 slice_convert_fusion.1
  31.4 0.1 reshape.88
  31.6 0.1 reshape.81
  31.7 1.4 %multiply_reduce_fusion = (f32[4,4]{1,0:T(4,128)S(1)}, f32[4,4,256]{2,1,0:T(4,128)}) fusion(f32[4,4,256]{2,1,0:T(4,128)S(1)} %mul.70, f32[4,4,256]{2,1,0:T(4,128)S(1)} %reshape.81, f32[4,4]{1,0:T(4,128)S(1)} %subtract_exponential_fusion, f32[4,4,256]{2,1,0:T(4,128)} %param.21, f32[4,4]{1,0:T(4,128)S(1)} %get-tuple-element.12), kind=kLoop, calls=%fused_computation.6 | loop fusion | flops 20464 | bytes 65728 | tf_op jit(solution)/shard_map/reduce_sum | solution.py:412
  33.1 0.1 reshape.95
  33.3 0.1 reshape.89
  33.5 0.1 reshape.82
  33.6 4.2 %multiply_add_fusion = f32[4,4,256,512]{3,2,1,0:T(8,128)S(1)} fusion(f32[4,4,256,512]{3,2,1,0:T(8,128)} %param.20, f32[4,4,512]{2,1,0:T(4,128)S(1)} %reshape.82, f32[4,4,256]{2,1,0:T(4,128)S(1)} %reshape.81, f32[4,4]{1,0:T(4,128)S(1)} %subtract_exponential_fusion, f32[4,4]{1,0:T(4,128)S(1)} %get-tuple-element.12), kind=kLoop, calls=%fused_computation | loop fusion | flops 8388608 | bytes 16826496 | tf_op jit(solution)/shard_map/add | solution.py:407
  37.8 0.0 copy-start.13
  37.8 0.0 copy-start.16
  37.9 4.0 %fusion.6 = f32[4,4,1,512]{3,2,1,0:T(1,128)S(1)} fusion(f32[4,4,256,1]{2,3,1,0:T(1,128)S(1)} %reshape.95, f32[4,4,256,512]{3,2,1,0:T(8,128)S(1)} %multiply_add_fusion), kind=kOutput, calls=%fused_computation.20 | convolution fusion | flops 25165824 | bytes 8437760 | tf_op jit(solution)/shard_map/shd,shde->she/dot_general | solution.py:411
  41.9 0.1 fusion.1
  42.0 0.1 select_reduce_fusion.route_ref
  42.1 0.9 %copy-done.1 = bf16[1,4096,256]{2,1,0:T(8,128)(2,1)S(1)} copy-done((bf16[1,4096,256]{2,1,0:T(8,128)(2,1)S(1)}, bf16[1,4096,256]{2,1,0:T(8,128)(2,1)}, u32[]{:S(2)}) %copy-start.1) | copy-done | bytes 2097176
  43.1 0.3 copy-done.4
  43.3 37.3 %ffn.1 = bf16[4,4096]{1,0:T(4,128)(2,1)S(1)} custom-call(bf16[4,2048]{1,0:T(4,128)(2,1)S(1)} %bitcast.52, bf16[4,4096]{1,0:T(4,128)(2,1)S(1)} %copy-done.8, f32[1,4096]{1,0:T(1,128)S(1)} %bitcast.56, f32[4,16]{1,0:T(4,128)S(1)} %select_reduce_fusion.route_ref, bf16[2048,256]{1,0:T(8,128)(2,1)S(1)} %copy-done.4, bf16[4096,256]{1,0:T(8,128)(2,1)S(1)} %bitcast.46, ...), custom_call_target="tpu_custom_call" | custom-call | tf_op jit(solution)/shard_map/ffn/pallas_call | solution.py:318
  80.7 0.6 copy.49
  (31 shorter events, 0.3 us)
Async XLA Ops:
  0.6 1.2 %copy-start.2 = (bf16[4096,4,32]{0,2,1:T(8,128)(2,1)S(1)}, bf16[4096,4,32]{0,2,1:T(8,128)(2,1)}, u32[]{:S(2)}) copy-start(bf16[4096,4,32]{0,2,1:T(8,128)(2,1)} %param.26) | copy-start | bytes 3145732
  1.9 1.2 %copy-start.3 = (bf16[4096,4,32]{0,2,1:T(8,128)(2,1)S(1)}, bf16[4096,4,32]{0,2,1:T(8,128)(2,1)}, u32[]{:S(2)}) copy-start(bf16[4096,4,32]{0,2,1:T(8,128)(2,1)} %param.27) | copy-start | bytes 3145732
  3.1 1.0 %copy-start.5 = (bf16[4096,4,16]{0,2,1:T(8,128)(2,1)S(1)}, bf16[4096,4,16]{0,2,1:T(8,128)(2,1)}, u32[]{:S(2)}) copy-start(bf16[4096,4,16]{0,2,1:T(8,128)(2,1)} %param.24) | copy-start | bytes 1572868
  4.1 1.0 %copy-start.6 = (bf16[4096,4,16]{0,2,1:T(8,128)(2,1)S(1)}, bf16[4096,4,16]{0,2,1:T(8,128)(2,1)}, u32[]{:S(2)}) copy-start(bf16[4096,4,16]{0,2,1:T(8,128)(2,1)} %param.25) | copy-start | bytes 1572868
  5.2 0.8 copy-start.7
  5.9 0.8 copy-start.9
  6.7 0.8 copy-start.10
  7.4 0.7 copy-start.11
  31.0 6.8 %copy-start.14 = (f32[4,4]{1,0:T(4,128)}, f32[4,4]{1,0:T(4,128)S(1)}, u32[]{:S(2)}) copy-start(f32[4,4]{1,0:T(4,128)S(1)} %get-tuple-element.21) | copy-start | bytes 196
  37.8 43.5 %copy-start.13 = (f32[4,4,256,512]{3,2,1,0:T(8,128)}, f32[4,4,256,512]{3,2,1,0:T(8,128)S(1)}, u32[]{:S(2)}) copy-start(f32[4,4,256,512]{3,2,1,0:T(8,128)S(1)} %multiply_add_fusion) | copy-start | bytes 25165828
  37.8 4.2 %copy-start.15 = (f32[4,2]{0,1:T(2,128)S(1)}, f32[4,2]{0,1:T(2,128)}, u32[]{:S(2)}) copy-start(f32[4,2]{0,1:T(2,128)} %param.37) | copy-start | bytes 100
  37.8 4.2 %copy-start.16 = (s32[4,2]{0,1:T(2,128)S(1)}, s32[4,2]{0,1:T(2,128)}, u32[]{:S(2)}) copy-start(s32[4,2]{0,1:T(2,128)} %param.36) | copy-start | bytes 100
  37.8 4.3 %copy-start = (bf16[1,4096,256]{2,1,0:T(8,128)(2,1)S(1)}, bf16[1,4096,256]{2,1,0:T(8,128)(2,1)}, u32[]{:S(2)}) copy-start(bf16[1,4096,256]{2,1,0:T(8,128)(2,1)} %param.33) | copy-start | bytes 6291460
  37.8 5.2 %copy-start.1 = (bf16[1,4096,256]{2,1,0:T(8,128)(2,1)S(1)}, bf16[1,4096,256]{2,1,0:T(8,128)(2,1)}, u32[]{:S(2)}) copy-start(bf16[1,4096,256]{2,1,0:T(8,128)(2,1)} %param.34) | copy-start | bytes 6291460
  37.8 5.5 %copy-start.4 = (bf16[2048,256]{1,0:T(8,128)(2,1)S(1)}, bf16[2048,256]{1,0:T(8,128)(2,1)}, u32[]{:S(2)}) copy-start(bf16[2048,256]{1,0:T(8,128)(2,1)} %wout_ref.1) | copy-start | bytes 3145732
  37.8 5.5 %copy-start.8 = (bf16[4,4096]{1,0:T(4,128)(2,1)S(1)}, bf16[4,4096]{1,0:T(4,128)(2,1)}, u32[]{:S(2)}) copy-start(bf16[4,4096]{1,0:T(4,128)(2,1)} %tokens_ref.3) | copy-start | bytes 98308
  37.9 5.5 %copy-start.12 = (f32[4096]{0:T(1024)S(1)}, f32[4096]{0:T(1024)}, u32[]{:S(2)}) copy-start(f32[4096]{0:T(1024)} %param.32) | copy-start | bytes 49156

commit v2 on v1

--- a/solution.py
+++ b/solution.py
@@ -9,6 +9,7 @@
 
 MESH = pl.DeviceIdType.MESH
 VMEM_LIMIT = 48 * 1024 * 1024
+VMEM_ALL = 67043328
 
 
 def product(left, right):
@@ -120,12 +121,20 @@
 
 def cell_in_kernel(
     n,
-    tokens_ref, gain_ref, win_ref, wforget_ref, wq_ref, wk_ref, wv_ref, wo_ref,
+    tokens_hbm, gain_hbm, win_hbm, wforget_hbm, wq_ref, wk_ref, wv_ref, wo_ref,
     inpre_ref, fpre_ref, proj_ref,
-    own, gathered, weights, rows_lo, rows_hi, outbox, inbox,
-    wsem, send, recv, rsend, rrecv, xsend, xrecv,
+    tokens_ref, gain_ref, win_ref, wforget_ref, own, gathered, weights, rows_lo, rows_hi, outbox, inbox,
+    ssem, wsem, send, recv, rsend, rrecv, xsend, xrecv,
 ):
     me, t = lax.axis_index("ep"), lax.axis_index("tp")
+    small = [
+        pltpu.make_async_copy(ref, dest, ssem.at[index])
+        for index, (ref, dest) in enumerate(
+            ((tokens_hbm, tokens_ref), (gain_hbm, gain_ref), (win_hbm, win_ref), (wforget_hbm, wforget_ref))
+        )
+    ]
+    for load in small:
+        load.start()
     loads, first = [], 0
     for index, ref in enumerate((wq_ref, wk_ref, wv_ref, wo_ref)):
         count = ref.shape[0]
@@ -139,6 +148,8 @@
 
     half = own.shape[2]
     seqs = own.shape[1]
+    for load in small:
+        load.wait()
     normed = rms_scale(tokens_ref[...].astype(jnp.float32), gain_ref[...]).astype(jnp.bfloat16)
     own[0] = normed[:, :half]
     own[1] = normed[:, half:]
@@ -235,12 +246,13 @@
     act = (jax.nn.silu(gate) * up).astype(jnp.bfloat16)
     loads[3].wait()
     width = min(512, half)
-    for index in range(2):
+    across = remote(terms.at[1 - t], other, tsend, trecv, (me, 1 - t))
+    for index in (1 - t, t):
         for first in range(0, half, width):
-            block = product(act, wdown[:, index * half + first : index * half + first + width])
+            block = product(act, wdown[:, pl.ds(pl.multiple_of(index * half + first, 128), width)])
             terms[index, :, first : first + width] = block.astype(jnp.bfloat16)
-    across = remote(terms.at[1 - t], other, tsend, trecv, (me, 1 - t))
-    across.start()
+        if index is not t:
+            across.start()
     across.wait_recv()
     rows = max(seqs, 16)
     for first in range(0, n * seqs, rows):
@@ -274,6 +286,10 @@
     return pl.BlockSpec(memory_space=pltpu.VMEM)
 
 
+def hbm_spec():
+    return pl.BlockSpec(memory_space=pltpu.MemorySpace.HBM)
+
+
 def any_spec():
     return pl.BlockSpec(memory_space=pl.ANY)
 
@@ -292,9 +308,13 @@
             jax.ShapeDtypeStruct((seqs, heads), jnp.float32),
             jax.ShapeDtypeStruct((n, seqs, columns), bf16),
         ),
-        in_specs=[vmem_spec()] * 4 + [any_spec()] * 4,
+        in_specs=[hbm_spec()] * 8,
         out_specs=(vmem_spec(),) * 3,
         scratch_shapes=[
+            pltpu.VMEM((seqs, width), bf16),
+            pltpu.VMEM((1, width), jnp.float32),
+            pltpu.VMEM((heads, width), bf16),
+            pltpu.VMEM((heads, width), bf16),
             pltpu.VMEM((2, seqs, width // 2), bf16),
             pltpu.VMEM((n, 2, seqs, width // 2), bf16),
             pltpu.VMEM((columns, width), bf16),
@@ -303,9 +323,10 @@
             pltpu.VMEM((n, seqs, columns), bf16),
             pltpu.VMEM((n, seqs, columns), bf16),
             dma((4,)),
+            dma((4,)),
         ]
         + [dma((n,))] * 6,
-        compiler_params=pltpu.CompilerParams(collective_id=0, has_side_effects=True, vmem_limit_bytes=VMEM_LIMIT),
+        compiler_params=pltpu.CompilerParams(collective_id=0, has_side_effects=True, vmem_limit_bytes=VMEM_ALL),
         name="cell_in",
     )(tokens, gain.reshape(1, width), w_input.T, w_forget.T, *flat)
 

time: 81.9 us -> 78 us (0.952)
  local copies, waits for them, and re-layouts: 10.6 us -> 3.12 us
  other arithmetic: 6.59 us -> 10.1 us
    unnamed x36 -> x20, local copies, waits for them, and re-layouts: 9.39 us -> 1.88 us
    convert_element_type x2, other arithmetic: 0.09 us -> 1.52 us  [split(): jnp.transpose(part, (1, 2, 0, 3)).reshape(seqs, heads, n * piece)]
where the time goes in v2:
time: 78 us; the launch traced here: 77.6 us
  Pallas kernels  59.4 us (76%)
  other arithmetic  10.1 us (13%)
  matrix products  4.05 us (5%)
  local copies, waits for them, and re-layouts  3.12 us (4%)
  between operations  0.85 us (1%)
    pallas_call x1, Pallas kernels, ffn(): pl.pallas_call(functools.partial(ffn_kernel, n), out_shape=jax.ShapeDtype...  37.2 us
    pallas_call x1, Pallas kernels, cell_in(): pl.pallas_call(functools.partial(cell_in_kernel, n), out_shape=(jax.Shape...  22.3 us
    add x1, other arithmetic, body(): decay[:, :, None, None] * memory  4.18 us
    dot_general x1, matrix products, body(): jnp.einsum('shd,shde->she', scaled, memory_next, precision=lax.Precision....  4.05 us
    unnamed x20, local copies, waits for them, and re-layouts  1.88 us

profile of v2, /device:TPU:1, one launch (start us, length us, event | category | flops | bytes accessed | tf_op | source)
XLA Modules:
  0.0 77.6 jit_solution(2489334943715834897)
XLA Ops:
  0.6 22.3 %cell_in.1 = (f32[4,4]{1,0:T(4,128)}, f32[4,4]{1,0:T(4,128)}, bf16[16,4,384]{2,1,0:T(4,128)(2,1)}) custom-call(bf16[4,4096]{1,0:T(4,128)(2,1)} %tokens_ref.1, f32[1,4096]{1,0:T(1,128)} %bitcast.61, bf16[4,4096]{1,0:T(4,128)(2,1)} %bitcast.59, bf16[4,4096]{1,0:T(4,128)(2,1)} %bitcast.60, bf16[64,4096]{1,0:T(8,128)(2,1)} %bitcast.53, ...), custom_call_target="tpu_custom_call" | custom-call | tf_op jit(solution)/shard_map/cell_in/pallas_call | solution.py:304
  22.9 0.7 add_divide_fusion
  23.7 0.1 reshape.91
  23.8 0.1 reshape.85
  24.0 0.7 subtract_exponential_fusion.1
  24.7 0.0 copy-start.6
  24.7 0.7 convert_multiply_fusion
  25.4 0.1 mul.68
  25.6 0.1 mul.70
  25.7 0.8 %slice_convert_fusion.1 = f32[16,4,64]{2,1,0:T(4,128)S(1)} fusion(bf16[16,4,384]{2,1,0:T(4,128)(2,1)} %get-tuple-element.7), kind=kLoop, calls=%fused_computation.9 | loop fusion | flops 4096 | bytes 24576 | tf_op jit(solution)/shard_map/convert_element_type | solution.py:419
  26.5 0.1 reshape.88
  26.7 0.1 reshape.81
  26.8 0.7 subtract_exponential_fusion
  27.5 1.4 %multiply_reduce_fusion = (f32[4,4]{1,0:T(4,128)S(1)}, f32[4,4,256]{2,1,0:T(4,128)}) fusion(f32[4,4,256]{2,1,0:T(4,128)S(1)} %mul.70, f32[4,4,256]{2,1,0:T(4,128)S(1)} %reshape.81, f32[4,4]{1,0:T(4,128)S(1)} %subtract_exponential_fusion, f32[4,4,256]{2,1,0:T(4,128)} %param.21, f32[4,4]{1,0:T(4,128)S(1)} %get-tuple-element.12), kind=kLoop, calls=%fused_computation.6 | loop fusion | flops 20464 | bytes 65728 | tf_op jit(solution)/shard_map/reduce_sum | solution.py:433
  28.9 0.1 reshape.95
  29.0 0.7 slice_convert_fusion
  29.7 0.1 reshape.89
  29.9 0.1 reshape.82
  30.0 4.2 %multiply_add_fusion = f32[4,4,256,512]{3,2,1,0:T(8,128)S(1)} fusion(f32[4,4,256,512]{3,2,1,0:T(8,128)} %param.20, f32[4,4,512]{2,1,0:T(4,128)S(1)} %reshape.82, f32[4,4,256]{2,1,0:T(4,128)S(1)} %reshape.81, f32[4,4]{1,0:T(4,128)S(1)} %subtract_exponential_fusion, f32[4,4]{1,0:T(4,128)S(1)} %get-tuple-element.12), kind=kLoop, calls=%fused_computation | loop fusion | flops 8388608 | bytes 16826496 | tf_op jit(solution)/shard_map/add | solution.py:428
  34.2 0.0 copy-start.5
  34.2 0.0 copy-start.7
  34.2 0.0 copy-start.8
  34.3 0.0 copy-start
  34.3 0.0 copy-start.1
  34.3 0.0 copy-start.4
  34.3 4.0 %fusion.6 = f32[4,4,1,512]{3,2,1,0:T(1,128)S(1)} fusion(f32[4,4,256,1]{2,3,1,0:T(1,128)S(1)} %reshape.95, f32[4,4,256,512]{3,2,1,0:T(8,128)S(1)} %multiply_add_fusion), kind=kOutput, calls=%fused_computation.20 | convolution fusion | flops 25165824 | bytes 8437760 | tf_op jit(solution)/shard_map/shd,shde->she/dot_general | solution.py:432
  38.4 0.1 fusion.1
  38.5 0.1 select_reduce_fusion.route_ref
  38.6 0.9 %copy-done.1 = bf16[1,4096,256]{2,1,0:T(8,128)(2,1)S(1)} copy-done((bf16[1,4096,256]{2,1,0:T(8,128)(2,1)S(1)}, bf16[1,4096,256]{2,1,0:T(8,128)(2,1)}, u32[]{:S(2)}) %copy-start.1) | copy-done | bytes 2097176
  39.5 0.3 copy-done.2
  39.8 37.2 %ffn.1 = bf16[4,4096]{1,0:T(4,128)(2,1)S(1)} custom-call(bf16[4,2048]{1,0:T(4,128)(2,1)S(1)} %bitcast.48, bf16[4,4096]{1,0:T(4,128)(2,1)S(1)} %copy-done.3, f32[1,4096]{1,0:T(1,128)S(1)} %bitcast.49, f32[4,16]{1,0:T(4,128)S(1)} %select_reduce_fusion.route_ref, bf16[2048,256]{1,0:T(8,128)(2,1)S(1)} %copy-done.2, bf16[4096,256]{1,0:T(8,128)(2,1)S(1)} %bitcast.46, ...), custom_call_target="tpu_custom_call" | custom-call | tf_op jit(solution)/shard_map/ffn/pallas_call | solution.py:339
  77.0 0.6 copy.49
  (15 shorter events, 0.2 us)
Async XLA Ops:
  24.7 9.5 %copy-start.6 = (f32[4,4]{1,0:T(4,128)}, f32[4,4]{1,0:T(4,128)S(1)}, u32[]{:S(2)}) copy-start(f32[4,4]{1,0:T(4,128)S(1)} %get-tuple-element.21) | copy-start | bytes 196
  34.2 43.4 %copy-start.5 = (f32[4,4,256,512]{3,2,1,0:T(8,128)}, f32[4,4,256,512]{3,2,1,0:T(8,128)S(1)}, u32[]{:S(2)}) copy-start(f32[4,4,256,512]{3,2,1,0:T(8,128)S(1)} %multiply_add_fusion) | copy-start | bytes 25165828
  34.2 4.2 %copy-start.7 = (f32[4,2]{0,1:T(2,128)S(1)}, f32[4,2]{0,1:T(2,128)}, u32[]{:S(2)}) copy-start(f32[4,2]{0,1:T(2,128)} %param.37) | copy-start | bytes 100
  34.2 4.2 %copy-start.8 = (s32[4,2]{0,1:T(2,128)S(1)}, s32[4,2]{0,1:T(2,128)}, u32[]{:S(2)}) copy-start(s32[4,2]{0,1:T(2,128)} %param.36) | copy-start | bytes 100
  34.3 4.3 %copy-start = (bf16[1,4096,256]{2,1,0:T(8,128)(2,1)S(1)}, bf16[1,4096,256]{2,1,0:T(8,128)(2,1)}, u32[]{:S(2)}) copy-start(bf16[1,4096,256]{2,1,0:T(8,128)(2,1)} %param.33) | copy-start | bytes 6291460
  34.3 5.2 %copy-start.1 = (bf16[1,4096,256]{2,1,0:T(8,128)(2,1)S(1)}, bf16[1,4096,256]{2,1,0:T(8,128)(2,1)}, u32[]{:S(2)}) copy-start(bf16[1,4096,256]{2,1,0:T(8,128)(2,1)} %param.34) | copy-start | bytes 6291460
  34.3 5.5 %copy-start.2 = (bf16[2048,256]{1,0:T(8,128)(2,1)S(1)}, bf16[2048,256]{1,0:T(8,128)(2,1)}, u32[]{:S(2)}) copy-start(bf16[2048,256]{1,0:T(8,128)(2,1)} %wout_ref.1) | copy-start | bytes 3145732
  34.3 5.5 %copy-start.3 = (bf16[4,4096]{1,0:T(4,128)(2,1)S(1)}, bf16[4,4096]{1,0:T(4,128)(2,1)}, u32[]{:S(2)}) copy-start(bf16[4,4096]{1,0:T(4,128)(2,1)} %tokens_ref.1) | copy-start | bytes 98308
  34.3 5.5 %copy-start.4 = (f32[4096]{0:T(1024)S(1)}, f32[4096]{0:T(1024)}, u32[]{:S(2)}) copy-start(f32[4096]{0:T(1024)} %param.32) | copy-start | bytes 49156
